TPU v7x, 128 devices: a whole 4x4x4 slice. The times are simulated.
128 devices in a mesh: ep: 32 (over z, y, core), tp: 4 (over x).
Axes of the slice: x: 4, y: 4, z: 4, core: 2. Of those that a mesh axis runs over, the one named last changes fastest.
Arguments:
- queries: bfloat16 [16384, 1024], P('ep', 'tp'), may hold values from -6 to 6
- keys: bfloat16 [16384, 512], P('ep', 'tp'), may hold values from -6 to 6
- values: bfloat16 [16384, 512], P('ep', 'tp'), may hold values from -384 to 384
- query_gain: float32 [128], replicated, may hold values from 0.1 to 1.9
- key_gain: float32 [128], replicated, may hold values from 0.1 to 1.9
- out_proj: bfloat16 [1024, 2048], replicated, may hold values from -0.1875 to 0.1875
- tokens_b: bfloat16 [16384, 2048], P(('ep', 'tp')), may hold values from -6 to 6
- norm_gain: float32 [2048], replicated, may hold values from 0.1 to 1.9
- routes: int32 [16384, 2], P(('ep', 'tp')), may hold values from 0 to 127, all different within a row; in each aligned block of 128 rows (0 to 127, 128 to 255, ...) at most 4 rows name the same one
- group_prob: float32 [16384], P(('ep', 'tp')), may hold values from 0.25 to 1
- expert_logits: float32 [16384, 2], P(('ep', 'tp')), may hold values from -6 to 6
- w_gate: bfloat16 [128, 2048, 512], P(('ep', 'tp')), may hold values from -0.125 to 0.125
- w_up: bfloat16 [128, 2048, 512], P(('ep', 'tp')), may hold values from -0.125 to 0.125
- w_down: bfloat16 [128, 512, 2048], P(('ep', 'tp')), may hold values from -0.25 to 0.25
Outputs:
- mixed_a: bfloat16 [16384, 2048], P(('ep', 'tp'))
- mixed_b: bfloat16 [16384, 2048], P(('ep', 'tp'))
Inputs may be any that keep to these rules, and one draw needn't show every extreme that they name: Within the 128 rows of one device, no expert is named by more than 4 of the routes, and in every draw some expert is named exactly 4 times by the rows of some device. The 2 experts of a row differ.
All inputs are finite; a program needn't handle non-finite values.
Results may differ from a plain program's by a relative error of at most 0.014.
Values may be sent and summed in bfloat16 or wider, within the bound.
A program may use at most 128 MiB of HBM per device.

v0:
```python
import math

import jax
import jax.numpy as jnp
from jax import lax
from jax.sharding import PartitionSpec as P

GRID_W = 64


NORM_EPS = 1e-06
ROPE_BASE = 10000.0


def side_by_side(arrays, axis, dim, along):
    both = jnp.concatenate(arrays, axis=along)
    filled, at, finished = (lax.all_gather(both, axis, axis=dim, tiled=True), 0, [])
    for a in arrays:
        finished.append(lax.slice_in_dim(filled, at, at + a.shape[along], axis=along))
        at += a.shape[along]
    return tuple(finished)


def in_blocks(x, dim, size):
    before, after = (x.shape[:dim], x.shape[dim + 1 :])
    return jnp.moveaxis(x.reshape(*before, size, -1, *after), dim, 0)


def summed_on_arrival(x, axis, dim):
    tiles = in_blocks(x, dim, lax.axis_size(axis))
    arrived = lax.all_to_all(tiles, axis, split_axis=0, concat_axis=0, tiled=True)
    return arrived.astype(jnp.float32).sum(axis=0)


def rope_angles(row_count, offset, head_dim):
    quarter = head_dim // 4
    position = offset + jnp.arange(row_count, dtype=jnp.int32)
    grid_row = (position // GRID_W).astype(jnp.float32)
    grid_col = (position % GRID_W).astype(jnp.float32)
    frequency = ROPE_BASE ** (-jnp.arange(quarter, dtype=jnp.float32) / quarter)
    angles = jnp.concatenate([grid_row[:, None] * frequency, grid_col[:, None] * frequency], axis=1)
    return (jnp.cos(angles), jnp.sin(angles))


def norm_rotate(block_in, gain, cos_table, sin_table):
    wide = block_in.astype(jnp.float32)
    wide = wide * lax.rsqrt(jnp.mean(wide * wide, axis=-1, keepdims=True) + NORM_EPS) * gain
    half_width = wide.shape[-1] // 2
    first_half, second_half = (wide[..., :half_width], wide[..., half_width:])
    cos_b = cos_table[:, None, :]
    sin_b = sin_table[:, None, :]
    turned = jnp.concatenate(
        [first_half * cos_b - second_half * sin_b, second_half * cos_b + first_half * sin_b],
        axis=-1,
    )
    return turned.astype(jnp.bfloat16)


def attention_half(queries, keys, values, query_gain, key_gain, out_proj):
    row_count = queries.shape[0]
    head_dim = query_gain.shape[0]
    local_heads = queries.shape[1] // head_dim
    local_kv = keys.shape[1] // head_dim
    group_size = local_heads // local_kv
    offset = lax.axis_index("ep") * row_count
    cos_table, sin_table = rope_angles(row_count, offset, head_dim)
    qrot = norm_rotate(
        queries.reshape(row_count, local_heads, head_dim), query_gain, cos_table, sin_table
    )
    qrot = qrot.reshape(row_count, local_kv, group_size, head_dim)
    krot = norm_rotate(keys.reshape(row_count, local_kv, head_dim), key_gain, cos_table, sin_table)
    krot = krot.reshape(row_count, local_kv * head_dim)
    score_scale = head_dim ** (-0.5)
    start_pair = (
        jnp.zeros((row_count, local_kv, group_size, head_dim), jnp.float32),
        jnp.zeros((row_count, local_kv, group_size), jnp.float32),
    )
    key_piece, value_piece = side_by_side((krot, values), "ep", 0, 1)
    piece_rows = key_piece.shape[0]
    key_block = math.gcd(piece_rows, 1024)
    block_count = piece_rows // key_block
    key_tiles = key_piece.reshape(block_count, key_block, local_kv, head_dim)
    value_tiles = value_piece.reshape(block_count, key_block, local_kv, head_dim)

    def key_step(pair, tiles):
        numerator, denominator = pair
        key_tile, value_tile = tiles
        scores = (
            jnp.einsum("qhgd,khd->qhgk", qrot, key_tile, preferred_element_type=jnp.float32)
            * score_scale
        )
        weights = jnp.exp(scores).astype(jnp.bfloat16)
        denominator = denominator + jnp.sum(weights.astype(jnp.float32), axis=-1)
        numerator = numerator + jnp.einsum(
            "qhgk,khd->qhgd", weights, value_tile, preferred_element_type=jnp.float32
        )
        return ((numerator, denominator), None)

    numerator, denominator = lax.scan(key_step, start_pair, (key_tiles, value_tiles))[0]
    attended = (
        (numerator / denominator[..., None])
        .astype(jnp.bfloat16)
        .reshape(row_count, local_heads * head_dim)
    )
    own_width = local_heads * head_dim
    own_rows = lax.dynamic_slice_in_dim(out_proj, lax.axis_index("tp") * own_width, own_width, 0)
    return summed_on_arrival(
        jnp.dot(attended, own_rows, preferred_element_type=jnp.float32).astype(jnp.bfloat16),
        "tp",
        0,
    ).astype(jnp.bfloat16)


def expert_apply(inputs, gate_w, up_w, down_w):
    gate_part = jnp.dot(inputs, gate_w, preferred_element_type=jnp.float32)
    up_part = jnp.dot(inputs, up_w, preferred_element_type=jnp.float32)
    hidden = (jax.nn.silu(gate_part) * up_part).astype(jnp.bfloat16)
    return jnp.dot(hidden, down_w, preferred_element_type=jnp.float32).astype(jnp.bfloat16)


def expert_half(tokens_b, norm_gain, routes, group_prob, expert_logits, w_gate, w_up, w_down):
    ep_count = lax.axis_size("ep")
    tp_count = lax.axis_size("tp")
    device_count = ep_count * tp_count
    row_count, top_count = routes.shape
    model_width = tokens_b.shape[1]
    capacity = 2 * top_count * row_count // device_count
    wide_b = tokens_b.astype(jnp.float32)
    normed = (
        wide_b * lax.rsqrt(jnp.mean(wide_b * wide_b, axis=-1, keepdims=True) + NORM_EPS) * norm_gain
    ).astype(jnp.bfloat16)
    flat_routes = routes.reshape(-1)
    onehot = (flat_routes[:, None] == jnp.arange(device_count, dtype=jnp.int32)[None, :]).astype(
        jnp.int32
    )
    slot_rank = jnp.sum((jnp.cumsum(onehot, axis=0) - onehot) * onehot, axis=1)
    target_slot = flat_routes * capacity + slot_rank
    token_index = jnp.arange(row_count * top_count, dtype=jnp.int32) // top_count
    sender = (
        jnp.zeros((device_count * capacity, model_width), jnp.bfloat16)
        .at[target_slot]
        .set(normed[token_index])
    )
    arrived = lax.all_to_all(
        sender.reshape(device_count, capacity, model_width),
        ("ep", "tp"),
        split_axis=0,
        concat_axis=0,
        tiled=True,
    )
    expert_out = expert_apply(
        arrived.reshape(device_count * capacity, model_width), w_gate[0], w_up[0], w_down[0]
    )
    returned = lax.all_to_all(
        expert_out.reshape(device_count, capacity, model_width),
        ("ep", "tp"),
        split_axis=0,
        concat_axis=0,
        tiled=True,
    )
    returned = returned.reshape(device_count * capacity, model_width)
    picked = returned[target_slot].reshape(row_count, top_count, model_width).astype(jnp.float32)
    combine = group_prob[:, None] * jax.nn.softmax(expert_logits, axis=-1)
    return jnp.sum(picked * combine[:, :, None], axis=1).astype(jnp.bfloat16)


def body(
    queries,
    keys,
    values,
    query_gain,
    key_gain,
    out_proj,
    tokens_b,
    norm_gain,
    routes,
    group_prob,
    expert_logits,
    w_gate,
    w_up,
    w_down,
):
    mixed_a = attention_half(queries, keys, values, query_gain, key_gain, out_proj)
    mixed_b = expert_half(
        tokens_b, norm_gain, routes, group_prob, expert_logits, w_gate, w_up, w_down
    )
    return (mixed_a, mixed_b)


def solution(mesh):
    placed = (
        P("ep", "tp"),
        P("ep", "tp"),
        P("ep", "tp"),
        P(),
        P(),
        P(),
        P(("ep", "tp"), None),
        P(),
        P(("ep", "tp"), None),
        P(("ep", "tp")),
        P(("ep", "tp"), None),
        P(("ep", "tp"), None, None),
        P(("ep", "tp"), None, None),
        P(("ep", "tp"), None, None),
    )
    return jax.shard_map(
        body,
        mesh=mesh,
        in_specs=placed,
        out_specs=(P(("ep", "tp"), None), P(("ep", "tp"), None)),
        check_vma=False,
    )
```

profile of v0, /device:TPU:0, one launch (start us, length us, event | category | flops | bytes accessed | tf_op | source)
XLA Modules:
  0.0 193.5 jit_solution(17601214981905461361)
XLA Ops:
  12.7 7.0 %scatter_custom_fusion = bf16[512,2048]{1,0:T(8,128)(2,1)} fusion(s32[256]{0:T(256)S(1)} %bitcast.121, bf16[128,2048]{1,0:T(8,128)(2,1)S(1)} %fusion.28, s32[1024]{0:T(1024)S(1)} %pad_clamp_fusion.1, bf16[]{:T(256)} %constant.103.clone.1), kind=kCustom, calls=%fused_computation.32 | custom fusion | bytes 2097154 | tf_op jit(solution)/shard_map/scatter | solution.py:142
  19.7 4.2 %reshape.419 = bf16[128,4,2048]{2,1,0:T(4,128)(2,1)} reshape(bf16[512,2048]{1,0:T(8,128)(2,1)} %scatter_custom_fusion) | data formatting | bytes 4194304 | tf_op jit(solution)/shard_map/reshape | solution.py:145
  23.9 11.9 %all-to-all-start.1 = ((bf16[128,4,2048]{2,1,0:T(4,128)(2,1)}), bf16[128,4,2048]{2,1,0:T(4,128)(2,1)}, u32[]{:S(2)}, u32[]{:S(2)}) async-start(bf16[128,4,2048]{2,1,0:T(4,128)(2,1)} %reshape.419), calls=%async_computation.1 | async-start | bytes 4194304 | tf_op jit(solution)/shard_map/all_to_all | solution.py:144
  37.0 28.3 %all-to-all-done.1 = bf16[128,4,2048]{2,1,0:T(4,128)(2,1)} async-done(((bf16[128,4,2048]{2,1,0:T(4,128)(2,1)}), bf16[128,4,2048]{2,1,0:T(4,128)(2,1)}, u32[]{:S(2)}, u32[]{:S(2)}) %all-to-all-start.1) | async-done | bytes 2097184 | tf_op jit(solution)/shard_map/all_to_all | solution.py:144
  65.3 4.0 %reshape.420 = bf16[512,2048]{1,0:T(8,128)(2,1)} reshape(bf16[128,4,2048]{2,1,0:T(4,128)(2,1)} %all-to-all-done.1) | data formatting | bytes 4194304 | tf_op jit(solution)/shard_map/reshape | solution.py:152
  69.3 4.7 %fusion.18 = f32[512,512]{1,0:T(8,128)} fusion(bf16[512,2048]{1,0:T(8,128)(2,1)} %reshape.420, bf16[1,2048,512]{2,1,0:T(8,128)(2,1)} %param.27), kind=kOutput, calls=%fused_computation.22 | convolution fusion | flops 1073741824 | bytes 5242880 | tf_op jit(solution)/shard_map/dot_general | solution.py:115
  74.0 6.5 %convolution_convert_fusion.1 = bf16[512,2048]{1,0:T(8,128)(2,1)} fusion(bf16[1,512,2048]{2,1,0:T(8,128)(2,1)S(1)} %copy-done, bf16[512,2048]{1,0:T(8,128)(2,1)} %reshape.420, bf16[1,2048,512]{2,1,0:T(8,128)(2,1)} %param.28, f32[512,512]{1,0:T(8,128)} %fusion.18), kind=kOutput, calls=%fused_computation.18 | convolution fusion | flops 2150105088 | bytes 9437184 | tf_op jit(solution)/shard_map/dot_general | solution.py:118
  80.5 4.1 %reshape.421 = bf16[128,4,2048]{2,1,0:T(4,128)(2,1)} reshape(bf16[512,2048]{1,0:T(8,128)(2,1)} %convolution_convert_fusion.1) | data formatting | bytes 4194304 | tf_op jit(solution)/shard_map/reshape | solution.py:155
  84.6 6.3 %all-to-all-start.2 = ((bf16[128,4,2048]{2,1,0:T(4,128)(2,1)}), bf16[128,4,2048]{2,1,0:T(4,128)(2,1)}, u32[]{:S(2)}, u32[]{:S(2)}) async-start(bf16[128,4,2048]{2,1,0:T(4,128)(2,1)} %reshape.421), calls=%async_computation.2 | async-start | bytes 4194304 | tf_op jit(solution)/shard_map/all_to_all | solution.py:154
  90.9 5.7 %fusion.64 = (bf16[16384,128]{1,0:T(8,128)(2,1)}, bf16[16384,128]{1,0:T(8,128)(2,1)}) fusion(bf16[16384,256]{1,0:T(8,128)(2,1)} %all-gather.2.cloned.1.call-done), kind=kLoop, calls=%fused_computation.107 | loop fusion | bytes 16777216 | tf_op jit(solution)/shard_map/slice | solution.py:19
  96.7 52.8 %while.13 = (s32[]{:T(128)}, f32[512,1,2,128]{0,3,2,1:T(8,128)S(1)}, f32[512,1,2]{0,2,1:T(2,128)S(1)}, bf16[16,1024,1,128]{3,1,0,2:T(8,128)(2,1)}, bf16[16,1024,...) while((s32[]{:T(128)}, ...), condition=%wide.region_4.5_spmd.clone, body=%wide.region_2.4_spmd.clone.sunk | while | flops 541328384 | bytes 6045808 | solution.py:99
  103.2 1.8 convert_reduce_fusion.2
  109.8 1.8 convert_reduce_fusion.2
  116.4 1.8 convert_reduce_fusion.2
  123.1 1.8 convert_reduce_fusion.2
  129.7 1.8 convert_reduce_fusion.2
  149.5 3.3 %convolution_convert_fusion = bf16[512,2048]{1,0:T(8,128)(2,1)} fusion(bf16[512,256]{0,1:T(8,128)(2,1)S(1)} %bitcast.115, bf16[1024,2048]{1,0:T(8,128)(2,1)} %param.21, s32[]{:T(128)S(6)} %select_n.58), kind=kOutput, calls=%fused_computation.17 | convolution fusion | flops 537919488 | bytes 3407876 | tf_op jit(solution)/shard_map/dot_general | solution.py:108
  152.9 4.8 %all-to-all-start = ((bf16[4,128,2048]{2,1,0:T(8,128)(2,1)}), bf16[4,128,2048]{2,1,0:T(8,128)(2,1)}, u32[]{:S(2)}, u32[]{:S(2)}) async-start(bf16[4,128,2048]{2,1,0:T(8,128)(2,1)} %bitcast.112), calls=%async_computation | async-start | bytes 4194304 | tf_op jit(solution)/shard_map/all_to_all | solution.py:31
  157.9 4.0 %reshape.422 = bf16[512,2048]{1,0:T(8,128)(2,1)} reshape(bf16[128,4,2048]{2,1,0:T(4,128)(2,1)} %all-to-all-done.2) | data formatting | bytes 4194304 | tf_op jit(solution)/shard_map/reshape | solution.py:161
  161.8 4.2 %gather_fusion = bf16[256,2048]{1,0:T(8,128)(2,1)S(1)} fusion(bf16[512,2048]{1,0:T(8,128)(2,1)} %reshape.422, s32[1024]{0:T(1024)S(1)} %pad_clamp_fusion), kind=kCustom, calls=%fused_computation.1 | custom fusion | bytes 2098176 | tf_op jit(solution)/shard_map/gather | solution.py:162
  166.1 2.3 %reshape.424 = f32[128,2,2048]{2,1,0:T(2,128)} reshape(bf16[256,2048]{1,0:T(8,128)(2,1)S(1)} %gather_fusion) | data formatting | bytes 3145728 | tf_op jit(solution)/shard_map/convert_element_type | solution.py:162
  168.4 5.6 %multiply_reduce_fusion = bf16[128,2048]{1,0:T(8,128)(2,1)} fusion(f32[128,2,2048]{2,1,0:T(2,128)} %reshape.424, f32[128,2]{1,0:T(8,128)S(1)} %copy.44), kind=kLoop, calls=%fused_computation.24 | loop fusion | flops 786432 | bytes 2622464 | tf_op jit(solution)/shard_map/reduce_sum | solution.py:164
  174.0 9.8 %all-to-all-done = bf16[4,128,2048]{2,1,0:T(8,128)(2,1)} async-done(((bf16[4,128,2048]{2,1,0:T(8,128)(2,1)}), bf16[4,128,2048]{2,1,0:T(8,128)(2,1)}, u32[]{:S(2)}, u32[]{:S(2)}) %all-to-all-start) | async-done | bytes 2097184 | tf_op jit(solution)/shard_map/all_to_all | solution.py:31
  183.8 2.9 %reduce_sum.81 = bf16[128,2048]{1,0:T(8,128)(2,1)} reduce(bf16[4,128,2048]{2,1,0:T(8,128)(2,1)} %all-to-all-done, bf16[]{:T(256)} %constant.103.clone.1), dimensions={0}, to_apply=%region_5.6 | reduce | flops 786432 | bytes 2621442 | tf_op jit(solution)/shard_map/reduce_sum | solution.py:32
  (113 shorter events, 50.1 us)
Async XLA Ops:
  7.2 66.8 %copy-start = (bf16[1,512,2048]{2,1,0:T(8,128)(2,1)S(1)}, bf16[1,512,2048]{2,1,0:T(8,128)(2,1)}, u32[]{:S(2)}) copy-start(bf16[1,512,2048]{2,1,0:T(8,128)(2,1)} %param.29) | copy-start | bytes 6291460
  7.2 3.0 %copy-start.3 = (bf16[512,128]{1,0:T(8,128)(2,1)S(1)}, bf16[512,128]{1,0:T(8,128)(2,1)}, u32[]{:S(2)}) copy-start(bf16[512,128]{1,0:T(8,128)(2,1)} %param.18) | copy-start | bytes 393220
  7.2 3.8 %copy-start.6 = (s32[128,2]{0,1:T(2,128)S(1)}, s32[128,2]{0,1:T(2,128)}, u32[]{:S(2)}) copy-start(s32[128,2]{0,1:T(2,128)} %param.24) | copy-start | bytes 3076
  7.2 83.7 %all-gather.2.cloned.1.call-start = ((), (), s32[]{:S(2)}) async-start(), calls=%async_computation.3 | async-start | bytes 8650752 | tf_op jit(solution)/shard_map/all_gather | solution.py:17
  7.3 5.0 %copy-start.1 = (bf16[128,2048]{1,0:T(8,128)(2,1)S(1)}, bf16[128,2048]{1,0:T(8,128)(2,1)}, u32[]{:S(2)}) copy-start(bf16[128,2048]{1,0:T(8,128)(2,1)} %param.22) | copy-start | bytes 1572868
  8.5 4.0 %copy-start.5 = (f32[2048]{0:T(1024)S(1)}, f32[2048]{0:T(1024)}, u32[]{:S(2)}) copy-start(f32[2048]{0:T(1024)} %param.23) | copy-start | bytes 24580
  23.9 11.9 %copy-start.2 = (bf16[512,256]{1,0:T(8,128)(2,1)S(1)}, bf16[512,256]{1,0:T(8,128)(2,1)}, u32[]{:S(2)}) copy-start(bf16[512,256]{1,0:T(8,128)(2,1)} %param.16) | copy-start | bytes 786436
  23.9 12.6 %copy-start.8 = (f32[128]{0:T(128)S(1)}, f32[128]{0:T(128)}, u32[]{:S(2)}) copy-start(f32[128]{0:T(128)} %param.19) | copy-start | bytes 1540
  23.9 41.3 %all-to-all-start.1 = ((bf16[128,4,2048]{2,1,0:T(4,128)(2,1)}), bf16[128,4,2048]{2,1,0:T(4,128)(2,1)}, u32[]{:S(2)}, u32[]{:S(2)}) async-start(bf16[128,4,2048]{2,1,0:T(4,128)(2,1)} %reshape.419), calls=%async_computation.1 | async-start | bytes 4194304 | tf_op jit(solution)/shard_map/all_to_all | solution.py:144
  84.6 68.3 %all-to-all-start.2 = ((bf16[128,4,2048]{2,1,0:T(4,128)(2,1)}), bf16[128,4,2048]{2,1,0:T(4,128)(2,1)}, u32[]{:S(2)}, u32[]{:S(2)}) async-start(bf16[128,4,2048]{2,1,0:T(4,128)(2,1)} %reshape.421), calls=%async_computation.2 | async-start | bytes 4194304 | tf_op jit(solution)/shard_map/all_to_all | solution.py:154
  152.9 4.8 %copy-start.4 = (f32[128,2]{0,1:T(2,128)S(1)}, f32[128,2]{0,1:T(2,128)}, u32[]{:S(2)}) copy-start(f32[128,2]{0,1:T(2,128)} %param.26) | copy-start | bytes 3076
  152.9 4.9 %copy-start.7 = (f32[128]{0:T(128)S(1)}, f32[128]{0:T(128)}, u32[]{:S(2)}) copy-start(f32[128]{0:T(128)} %param.25) | copy-start | bytes 1540
  152.9 30.9 %all-to-all-start = ((bf16[4,128,2048]{2,1,0:T(8,128)(2,1)}), bf16[4,128,2048]{2,1,0:T(8,128)(2,1)}, u32[]{:S(2)}, u32[]{:S(2)}) async-start(bf16[4,128,2048]{2,1,0:T(8,128)(2,1)} %bitcast.112), calls=%async_computation | async-start | bytes 4194304 | tf_op jit(solution)/shard_map/all_to_all | solution.py:31
Sparse Core Ops, SparseCore 0:
  11.1 69.8 all-gather.1
where the time goes:
time: 195 us; the launch traced here: 194 us
  matrix products  66.6 us (34%)
  local copies, waits for them, and re-layouts  38.2 us (20%)
  waiting for transfers between devices  38.1 us (20%)
  starting transfers between devices  23.1 us (12%)
  between operations  14.4 us (7%)
  other arithmetic  12.7 us (7%)
    dot_general x16, matrix products, key_step(): jnp.einsum('qhgd,khd->qhgk', qrot, key_tile, preferred_element_type=jnp.f...  28.5 us
    all_to_all x1, waiting for transfers between devices, expert_half(): lax.all_to_all(sender.reshape(device_count, capacity, model_width), ('ep'...  28.3 us
    dot_general x16, matrix products, key_step(): jnp.einsum('qhgk,khd->qhgd', weights, value_tile, preferred_element_type=...  23.6 us
    all_to_all x1, starting transfers between devices, expert_half(): lax.all_to_all(sender.reshape(device_count, capacity, model_width), ('ep'...  11.9 us
    all_to_all x1, waiting for transfers between devices, summed_on_arrival(): lax.all_to_all(tiles, axis, split_axis=0, concat_axis=0, tiled=True)  9.76 us
    scatter x1, local copies, waits for them, and re-layouts, expert_half(): sender = jnp.zeros((device_count * capacity, model_width), jnp.bfloat16)....  7 us
    dot_general x1, matrix products, expert_apply(): jnp.dot(hidden, down_w, preferred_element_type=jnp.float32)  6.48 us
    all_to_all x1, starting transfers between devices, expert_half(): lax.all_to_all(expert_out.reshape(device_count, capacity, model_width), (...  6.32 us
  transfers between devices with their start and end apart: 4, of which 2 were waited for; matrix products, arithmetic and copies ran while one was open for 57% of the time, Pallas kernels for 0%

commit v1 on v0

v1 whole, which is shorter than its diff:
```python
import functools

import jax
import jax.numpy as jnp
import numpy as np
from jax import lax
from jax.experimental import pallas as pl
from jax.experimental.pallas import tpu as pltpu
from jax.sharding import PartitionSpec as P

GRID_W = 64
NORM_EPS = 1e-06
ROPE_BASE = 10000.0
HD = 128
CAP = 4
N_DEV = 128
ROWS = 512
TOK = 128
D = 2048
FF = 512
SEQ = 16384
SCALE_LOG2E = float(HD**-0.5 * np.log2(np.e))
KEY_BLOCK = 2048
MESH = pl.DeviceIdType.MESH
VMEM = pl.BlockSpec(memory_space=pltpu.VMEM)
ANY = pl.BlockSpec(memory_space=pl.ANY)


def angle_tables():
    quarter = HD // 4
    freq = (ROPE_BASE ** (-np.arange(quarter, dtype=np.float64) / quarter)).astype(np.float32)

    def pair(count, at):
        angles = np.arange(count, dtype=np.float32)[:, None] * freq[None, :]
        cos = np.zeros((count, HD), np.float32)
        sin = np.zeros((count, HD), np.float32)
        c, s = np.cos(angles.astype(np.float64)), np.sin(angles.astype(np.float64))
        cos[:, at : at + quarter] = c
        cos[:, 64 + at : 64 + at + quarter] = c
        sin[:, at : at + quarter] = -s
        sin[:, 64 + at : 64 + at + quarter] = s
        return cos, sin

    return pair(SEQ // GRID_W, 0) + pair(GRID_W, quarter)


def prep_kernel(
    q_ref, k_ref, v_ref, qg_ref, kg_ref, rc_ref, rs_ref, cc_ref, cs_ref,
    tok_ref, ng_ref, routes_ref, gp_ref, lg_ref,
    rows_ref, kv_ref, qr_ref, c0_ref, c1_ref, w_ref,
):
    f32, bf16 = jnp.float32, jnp.bfloat16
    wide = tok_ref[...].astype(f32)
    normed = (
        wide * lax.rsqrt(jnp.mean(wide * wide, axis=-1, keepdims=True) + NORM_EPS) * ng_ref[...]
    ).astype(bf16)
    lane = lax.broadcasted_iota(jnp.int32, (TOK, N_DEV), 1)
    sub = lax.broadcasted_iota(jnp.int32, (TOK, N_DEV), 0)
    r0, r1 = routes_ref[:, 0:1], routes_ref[:, 1:2]
    hot0 = (lane == r0).astype(f32)
    hot1 = (lane == r1).astype(f32)
    before = (sub > lane).astype(bf16)
    count0 = jnp.dot(before, hot0.astype(bf16), preferred_element_type=f32)
    count1 = jnp.dot(before, hot1.astype(bf16), preferred_element_type=f32)
    count1 = count1 + jnp.sum(hot0, axis=0, keepdims=True)
    rank0 = jnp.sum(count0 * hot0, axis=1, keepdims=True)
    rank1 = jnp.sum(count1 * hot1, axis=1, keepdims=True)
    slot0 = r0 * CAP + rank0.astype(jnp.int32)
    slot1 = r1 * CAP + rank1.astype(jnp.int32)
    slots = lax.broadcasted_iota(jnp.int32, (TOK, N_DEV * CAP), 1)
    c0 = (slots == slot0).astype(f32)
    c1 = (slots == slot1).astype(f32)
    c0_ref[...] = c0.astype(bf16)
    c1_ref[...] = c1.astype(bf16)
    picked = lax.dot_general(
        (c0 + c1).astype(bf16), normed, (((0,), (0,)), ((), ())), preferred_element_type=f32
    ).astype(bf16)
    rows_ref[...] = picked.reshape(N_DEV, CAP, D)

    l0, l1 = lg_ref[:, 0:1], lg_ref[:, 1:2]
    top = jnp.maximum(l0, l1)
    e0, e1 = jnp.exp(l0 - top), jnp.exp(l1 - top)
    prob = jnp.sum(jnp.where(sub == lane, gp_ref[...], 0.0), axis=1, keepdims=True)
    w_ref[:, 0:1] = prob * (e0 / (e0 + e1))
    w_ref[:, 1:2] = prob * (e1 / (e0 + e1))

    ep = lax.axis_index("ep")
    grid_rows = ROWS // GRID_W
    here = pl.ds(pl.multiple_of(ep * grid_rows, grid_rows), grid_rows)
    cos = (rc_ref[here, :][:, None, :] + cc_ref[...][None, :, :]).reshape(ROWS, HD)
    sin = (rs_ref[here, :][:, None, :] + cs_ref[...][None, :, :]).reshape(ROWS, HD)

    def turned(x, gain):
        x = x.astype(f32)
        x = x * lax.rsqrt(jnp.mean(x * x, axis=-1, keepdims=True) + NORM_EPS) * gain
        return (x * cos + pltpu.roll(x, 64, 1) * sin).astype(bf16)

    kv_ref[:, :HD] = turned(k_ref[...], kg_ref[...])
    kv_ref[:, HD:] = v_ref[...]
    qr_ref[:ROWS] = turned(q_ref[:, :HD], qg_ref[...])
    qr_ref[ROWS:] = turned(q_ref[:, HD:], qg_ref[...])


def arrivals():
    def of(o1, o2):
        parts = (0, 1) if (o1 == 2 or o2 == 2) else (None,)
        return [(p, o1, o2, part) for p in (0, 1) for part in parts]

    order = []
    for o1, o2 in [
        (-1, 0), (1, 0), (0, -1), (0, 1), (2, 0),
        (-1, -1), (1, 1), (-1, 1), (1, -1), (0, 2),
        (2, -1), (2, 1), (-1, 2), (1, 2), (2, 2),
    ]:
        order += of(o1, o2)
    return order


ARRIVALS = arrivals()
SEM_OF = {a: i for i, a in enumerate(ARRIVALS)}


def main_kernel(
    rows_ref, kv_ref, qr_ref, c0_ref, c1_ref, w_ref, wg_hbm, wu_hbm, wd_hbm, op_hbm,
    a_ref, b_ref,
    kvbuf, arrived, sent, ret, acc, att_out, att_in, wg, wu, wd, op,
    w_sem, disp_send, disp_recv, ret_send, ret_recv, kv_send, kv_recv, d2d_send, d2d_recv,
    att_send, att_recv,
):
    f32, bf16 = jnp.float32, jnp.bfloat16
    ep, tp = lax.axis_index("ep"), lax.axis_index("tp")
    z, y, c = ep // 8, (ep // 2) % 4, ep % 2
    me = ep * 4 + tp
    g = (tp + y + z) % 4
    partner = ep + 1 - 2 * c

    loads = [
        pltpu.make_async_copy(wg_hbm.at[0], wg, w_sem.at[0]),
        pltpu.make_async_copy(wu_hbm.at[0], wu, w_sem.at[1]),
        pltpu.make_async_copy(wd_hbm.at[0], wd, w_sem.at[2]),
        pltpu.make_async_copy(op_hbm, op, w_sem.at[3]),
    ]
    for load in loads:
        load.start()

    def remote(src, dst, send, recv, to):
        return pltpu.make_async_remote_copy(
            src_ref=src, dst_ref=dst, send_sem=send, recv_sem=recv,
            device_id=to, device_id_type=MESH,
        )

    barrier = pltpu.get_barrier_semaphore()

    def greet(k, _):
        to = (ep ^ (k // 4), tp ^ (k % 4))
        pl.semaphore_signal(barrier, 1, device_id=to, device_id_type=MESH)
        return 0

    lax.fori_loop(1, N_DEV, greet, 0)

    own_rows = pl.ds(pl.multiple_of(ep * ROWS, ROWS), ROWS)
    kvbuf[own_rows, :] = kv_ref[...]
    arrived[g * 32 + ep] = rows_ref[me]
    pl.semaphore_wait(barrier, N_DEV - 1)

    def moved(p, ring, step):
        if (ring == 0) == (p == 0):
            return ((z * 4 + (y + step + 4) % 4) * 2 + c, tp)
        return ((((z + step + 4) % 4) * 4 + y) * 2 + c, tp)

    def owner_rows(p, o1, o2, part):
        dy, dz = (o1, o2) if p == 0 else (o2, o1)
        owner = (((z + dz + 4) % 4) * 4 + (y + dy + 4) % 4) * 2 + c
        start = owner * ROWS + p * 256 + (0 if part is None else part * 128)
        size = 256 if part is None else 128
        return pl.ds(pl.multiple_of(start, 128), size)

    def kv_copy(p, o1, o2, part, arrival, to, src=None):
        where = owner_rows(p, o1, o2, part)
        return remote(
            kvbuf.at[where] if src is None else src,
            kvbuf.at[where], kv_send, kv_recv.at[SEM_OF[arrival]], to,
        )

    def to_partner(p, o1, o2, part, sem, src=None):
        where = owner_rows(p, o1, o2, part)
        return remote(
            kvbuf.at[where] if src is None else src,
            kvbuf.at[where], d2d_send, d2d_recv.at[sem], (partner, tp),
        )

    def start_own():
        for p in (0, 1):
            half = kv_ref.at[pl.ds(p * 256, 256)]
            for ring in (0, 1):
                for step in (1, -1):
                    arrival = (p, -step, 0, None) if ring == 0 else (p, 0, -step, None)
                    kv_copy(p, 0, 0, None, arrival, moved(p, ring, step), half).start()
        for p in (0, 1):
            half = kv_ref.at[pl.ds(p * 256, 256)]
            to_partner(p, 0, 0, None, len(ARRIVALS) + p, half).start()

    def relay(a):
        p, o1, o2, part = a
        kv_copy(p, o1, o2, part, a, (partner, tp)).wait_recv()
        if o2 == 0 and o1 in (-1, 1):
            half = 0 if o1 == -1 else 1
            kv_copy(p, o1, 0, half, (p, 2, 0, half), moved(p, 0, -o1)).start()
        if o2 == 0:
            for step in (1, -1):
                kv_copy(p, o1, 0, part, (p, o1, -step, part), moved(p, 1, step)).start()
        if o2 in (-1, 1):
            half = 0 if o2 == -1 else 1
            if part is None or part == half:
                kv_copy(p, o1, o2, half, (p, o1, 2, half), moved(p, 1, -o2)).start()
        to_partner(p, o1, o2, part, SEM_OF[a]).start()

    def dispatch(jd, first, last):
        def send(m, _):
            k = (m * 11) % 32
            z2, y2, c2 = (z + k // 8) % 4, (y + (k // 2) % 4) % 4, (c + k % 2) % 2
            x2 = (g + jd + 8 - y2 - z2) % 4
            e2 = (z2 * 4 + y2) * 2 + c2
            remote(
                rows_ref.at[e2 * 4 + x2], arrived.at[g * 32 + ep],
                disp_send, disp_recv.at[(4 - jd) % 4], (e2, x2),
            ).start()
            return 0

        lax.fori_loop(first, last, send, 0)

    def experts(j):
        count = 31 if j == 0 else 32
        span = pl.ds(0, count)
        remote(
            rows_ref.at[span], arrived.at[span], disp_send, disp_recv.at[j], (partner, tp)
        ).wait_recv()
        group = (g + j) % 4
        at = pl.ds(pl.multiple_of(group * 32, 32), 32)
        x = arrived[at].reshape(32 * CAP, D)
        gate = jnp.dot(x, wg[...], preferred_element_type=f32)
        up = jnp.dot(x, wu[...], preferred_element_type=f32)
        hidden = (gate / (1.0 + jnp.exp(-gate)) * up).astype(bf16)
        out = jnp.dot(hidden, wd[...], preferred_element_type=f32).astype(bf16)
        sent[at] = out.reshape(32, CAP, D)

    def give_back(j):
        if j == 0:
            ret[me] = sent[g * 32 + ep]

        def send(m, _):
            k = (m * 11) % 32
            z2, y2, c2 = (z + k // 8) % 4, (y + (k // 2) % 4) % 4, (c + k % 2) % 2
            x2 = (g + j + 8 - y2 - z2) % 4
            e2 = (z2 * 4 + y2) * 2 + c2
            remote(
                sent.at[((g + j) % 4) * 32 + e2], ret.at[me], ret_send, ret_recv, (e2, x2)
            ).start()
            return 0

        lax.fori_loop(1 if j == 0 else 0, 32, send, 0)

    def attend(first, last):
        ones = jnp.ones((KEY_BLOCK, HD), bf16)

        def block(i, _):
            at = pl.ds(pl.multiple_of(i * KEY_BLOCK, KEY_BLOCK), KEY_BLOCK)
            key = kvbuf[at, :HD]
            value = jnp.concatenate([kvbuf[at, HD:], ones], axis=1)
            for t in range(4):
                rows = pl.ds(t * 256, 256)
                s = lax.dot_general(
                    qr_ref[rows], key, (((1,), (1,)), ((), ())), preferred_element_type=f32
                )
                weights = jnp.exp2(s * SCALE_LOG2E).astype(bf16)
                acc[rows] += jnp.dot(weights, value, preferred_element_type=f32)
            return 0

        lax.fori_loop(first, last, block, 0)

    start_own()
    for jd in (0, 3, 2, 1):
        dispatch(jd, 1 if jd == 0 else 0, 32)
    for a in ARRIVALS:
        relay(a)
    for load in loads[:3]:
        load.wait()
    for j in range(4):
        experts(j)
        give_back(j)
    for p in (0, 1):
        to_partner(p, 0, 0, None, len(ARRIVALS) + p).wait_recv()
    for a in ARRIVALS:
        p, o1, o2, part = a
        to_partner(p, o1, o2, part, SEM_OF[a]).wait_recv()
    acc[...] = jnp.zeros_like(acc)
    attend(0, SEQ // KEY_BLOCK)

    for t in range(4):
        for h in range(2):
            part = acc[pl.ds(h * ROWS + t * TOK, TOK)]
            att_out[t, :, h * HD : (h + 1) * HD] = (part[:, :HD] / part[:, HD:]).astype(bf16)
    for step in (1, 2, 3):
        to = (tp + step) % 4
        remote(att_out.at[to], att_in.at[tp], att_send, att_recv, (ep, to)).start()
    att_in[tp] = att_out[tp]
    loads[3].wait()
    span = pl.ds(0, 3)
    remote(att_out.at[span], att_in.at[span], att_send, att_recv, (partner, tp)).wait_recv()
    total = jnp.dot(att_in[0], op[0:256], preferred_element_type=f32)
    for t in range(1, 4):
        total += jnp.dot(att_in[t], op[t * 256 : (t + 1) * 256], preferred_element_type=f32)
    a_ref[...] = total.astype(bf16)

    span = pl.ds(0, N_DEV - 1)
    remote(sent.at[span], ret.at[span], ret_send, ret_recv, (partner, tp)).wait_recv()
    back = ret[...].reshape(N_DEV * CAP, D)
    first = jnp.dot(c0_ref[...], back, preferred_element_type=f32) * w_ref[:, 0:1]
    second = jnp.dot(c1_ref[...], back, preferred_element_type=f32) * w_ref[:, 1:2]
    b_ref[...] = (first + second).astype(bf16)

    remote(rows_ref.at[span], arrived.at[span], disp_send, ret_recv, (partner, tp)).wait_send()
    remote(sent.at[span], ret.at[span], ret_send, ret_recv, (partner, tp)).wait_send()
    remote(
        kvbuf.at[pl.ds(0, 15 * ROWS)], kvbuf.at[pl.ds(0, 15 * ROWS)],
        kv_send, kv_recv.at[0], (partner, tp),
    ).wait_send()
    remote(
        kvbuf.at[pl.ds(0, 16 * ROWS)], kvbuf.at[pl.ds(0, 16 * ROWS)],
        d2d_send, d2d_recv.at[0], (partner, tp),
    ).wait_send()
    three = pl.ds(0, 3)
    remote(att_out.at[three], att_in.at[three], att_send, att_recv, (partner, tp)).wait_send()


def body(
    queries, keys, values, query_gain, key_gain, out_proj, tokens_b, norm_gain, routes,
    group_prob, expert_logits, w_gate, w_up, w_down,
):
    bf16, f32 = jnp.bfloat16, jnp.float32
    tables = [jnp.asarray(t) for t in angle_tables()]
    out = jax.ShapeDtypeStruct
    rows, kv, qr, c0, c1, weight = pl.pallas_call(
        prep_kernel,
        out_shape=(
            out((N_DEV, CAP, D), bf16),
            out((ROWS, 2 * HD), bf16),
            out((2 * ROWS, HD), bf16),
            out((TOK, N_DEV * CAP), bf16),
            out((TOK, N_DEV * CAP), bf16),
            out((TOK, 2), f32),
        ),
        in_specs=[VMEM] * 14,
        out_specs=(VMEM,) * 6,
        compiler_params=pltpu.CompilerParams(vmem_limit_bytes=40 << 20),
    )(
        queries, keys, values, query_gain.reshape(1, HD), key_gain.reshape(1, HD), *tables,
        tokens_b, norm_gain.reshape(1, D), routes, group_prob.reshape(1, TOK), expert_logits,
    )
    dma, many = pltpu.SemaphoreType.DMA, len(ARRIVALS)
    return pl.pallas_call(
        main_kernel,
        out_shape=(out((TOK, D), bf16), out((TOK, D), bf16)),
        in_specs=[VMEM] * 6 + [ANY] * 4,
        out_specs=(VMEM, VMEM),
        scratch_shapes=[
            pltpu.VMEM((SEQ, 2 * HD), bf16),
            pltpu.VMEM((N_DEV, CAP, D), bf16),
            pltpu.VMEM((N_DEV, CAP, D), bf16),
            pltpu.VMEM((N_DEV, CAP, D), bf16),
            pltpu.VMEM((2 * ROWS, 2 * HD), f32),
            pltpu.VMEM((4, TOK, 2 * HD), bf16),
            pltpu.VMEM((4, TOK, 2 * HD), bf16),
            pltpu.VMEM((D, FF), bf16),
            pltpu.VMEM((D, FF), bf16),
            pltpu.VMEM((FF, D), bf16),
            pltpu.VMEM((8 * HD, D), bf16),
            dma((4,)), dma, dma((4,)), dma, dma, dma, dma((many,)), dma, dma((many + 2,)),
            dma, dma,
        ],
        compiler_params=pltpu.CompilerParams(
            collective_id=0, has_side_effects=True, vmem_limit_bytes=60 << 20
        ),
    )(rows, kv, qr, c0, c1, weight, w_gate, w_up, w_down, out_proj)


def solution(mesh):
    both = P(("ep", "tp"), None)
    placed = (
        P("ep", "tp"),
        P("ep", "tp"),
        P("ep", "tp"),
        P(),
        P(),
        P(),
        both,
        P(),
        both,
        P(("ep", "tp")),
        both,
        P(("ep", "tp"), None, None),
        P(("ep", "tp"), None, None),
        P(("ep", "tp"), None, None),
    )
    return jax.shard_map(
        body, mesh=mesh, in_specs=placed, out_specs=(both, both), check_vma=False
    )
```

time: 195 us -> 118 us (0.61)
  Pallas kernels: 0 us -> 97.4 us
  matrix products: 66.6 us -> 0 us
  waiting for transfers between devices: 38.1 us -> 0 us
  starting transfers between devices: 23.1 us -> 0 us
  local copies, waits for them, and re-layouts: 38.2 us -> 19.8 us
  between operations: 14.4 us -> 0.68 us
  other arithmetic: 12.7 us -> 0 us
    pallas_call x0 -> x2, Pallas kernels: none -> 97.4 us  [the longest x1 96 us: body(): pl.pallas_call(main_kernel, out_shape=(out((TOK, D), bf16), out((TOK, D),...]
    dot_general x35 -> x0, matrix products: 66.6 us -> none  [the longest x16 28.5 us: key_step(): jnp.einsum('qhgd,khd->qhgk', qrot, key_tile, preferred_element_type=jnp.f...]
    all_to_all x3 -> x0, waiting for transfers between devices: 38.1 us -> none  [the longest x1 28.3 us: expert_half(): lax.all_to_all(sender.reshape(device_count, capacity, model_width), ('ep'...]
    all_to_all x3 -> x0, starting transfers between devices: 23 us -> none  [the longest x1 11.9 us: expert_half(): lax.all_to_all(sender.reshape(device_count, capacity, model_width), ('ep'...]
    unnamed x23 -> x40, local copies, waits for them, and re-layouts: 1.63 us -> 19.8 us
    reshape x4 -> x0, local copies, waits for them, and re-layouts: 16.3 us -> none  [the longest x1 4.16 us: expert_half(): sender.reshape(device_count, capacity, model_width)]
    reduce_sum x7 -> x0, other arithmetic: 9.01 us -> none  [the longest x1 5.59 us: expert_half(): return jnp.sum(picked * combine[:, :, None], axis=1).astype(jnp.bfloat16)]
    scatter x1 -> x0, local copies, waits for them, and re-layouts: 7 us -> none  [expert_half(): sender = jnp.zeros((device_count * capacity, model_width), jnp.bfloat16)....]
  transfers between devices with their start and end apart: 4 -> 0, of which waited for: 2 -> 0; matrix products, arithmetic and copies ran while one was open for 57% -> 0% of each run, Pallas kernels for 0% -> 0%
where the time goes in v1:
time: 118 us
  Pallas kernels  97.4 us (83%)
  local copies, waits for them, and re-layouts  19.8 us (17%)
    pallas_call x1, Pallas kernels, body(): pl.pallas_call(main_kernel, out_shape=(out((TOK, D), bf16), out((TOK, D),...  96 us
    unnamed x40, local copies, waits for them, and re-layouts  19.8 us

profile of v1, /device:TPU:0, one launch (start us, length us, event | category | flops | bytes accessed | tf_op | source)
XLA Modules:
  0.0 117.8 jit_solution(8467070717260589898)
XLA Ops:
  0.6 0.8 copy.20.routes_ref
  1.4 0.8 copy.21.lg_ref
  2.2 1.0 copy-done.1
  3.2 0.9 copy-done.2
  4.2 0.9 copy-done.7
  5.1 0.9 copy-done.8
  6.0 0.9 copy-done.9
  6.9 0.9 copy-done.10
  7.8 0.8 copy-done.12
  8.6 0.8 copy-done.13
  9.3 0.7 copy-done.14
  10.0 0.7 copy-done.15
  10.7 0.7 copy-done.16
  11.3 0.7 copy-done.17
  12.0 1.4 %shard_map.185 = (bf16[128,4,2048]{2,1,0:T(4,128)(2,1)S(1)}, bf16[512,256]{1,0:T(8,128)(2,1)S(1)}, bf16[1024,128]{1,0:T(8,128)(2,1)S(1)}, bf16[128,512]{1,0:T(8,...) custom-call(bf16[512,256]{1,0:T(8,128)(2,1)S(1)} %copy-done.2, bf16[512,128]{1,0:T(8,128)(2,1)S(1)} %copy-done.7, ...), custom_call_target="tpu_custom_call" | custom-call | tf_op jit(solution)/shard_map/pallas_call | solution.py:343
  13.4 1.3 %copy-done = bf16[128,4,2048]{2,1,0:T(4,128)(2,1)} copy-done((bf16[128,4,2048]{2,1,0:T(4,128)(2,1)}, bf16[128,4,2048]{2,1,0:T(4,128)(2,1)S(1)}, u32[]{:S(2)}) %copy-start) | copy-done | bytes 2097176
  14.7 0.7 copy-done.3
  15.4 0.7 copy-done.4
  16.1 0.6 copy-done.5
  16.8 0.6 copy-done.6
  17.4 0.6 copy-done.11
  18.1 96.0 %shard_map.186 = (bf16[128,2048]{1,0:T(8,128)(2,1)}, bf16[128,2048]{1,0:T(8,128)(2,1)}) custom-call(bf16[128,4,2048]{2,1,0:T(4,128)(2,1)} %copy-done, bf16[512,256]{1,0:T(8,128)(2,1)} %copy-done.3, bf16[1024,128]{1,0:T(8,128)(2,1)} %copy-done.4, bf16[128,512]{1,0:T(8,128)(2,1)} %copy-done.5, bf16[128,512]{1,0:T(8,128)(2,1)} %copy-done.6, ...), custom_call_target="tpu_custom_call" | custom-call | tf_op jit(solution)/shard_map/pallas_call | solution.py:361
  114.1 1.9 %copy.24 = bf16[128,2048]{1,0:T(8,128)(2,1)} copy(bf16[128,2048]{1,0:T(8,128)(2,1)} %get-tuple-element.16) | data formatting | bytes 1048576
  116.0 1.9 %copy.25 = bf16[128,2048]{1,0:T(8,128)(2,1)} copy(bf16[128,2048]{1,0:T(8,128)(2,1)} %get-tuple-element.17) | data formatting | bytes 1048576
  (18 shorter events, 0.0 us)
Async XLA Ops:
  2.2 1.0 copy-start.1
  3.2 0.9 copy-start.2
  4.2 0.9 copy-start.7
  5.1 0.9 copy-start.8
  6.0 0.9 copy-start.9
  6.9 0.9 copy-start.10
  7.8 0.8 copy-start.12
  8.6 0.8 copy-start.13
  9.3 0.7 copy-start.14
  10.0 0.7 copy-start.15
  10.7 0.7 copy-start.16
  11.3 0.7 copy-start.17
  13.4 1.3 %copy-start = (bf16[128,4,2048]{2,1,0:T(4,128)(2,1)}, bf16[128,4,2048]{2,1,0:T(4,128)(2,1)S(1)}, u32[]{:S(2)}) copy-start(bf16[128,4,2048]{2,1,0:T(4,128)(2,1)S(1)} %get-tuple-element.8.rows_ref) | copy-start | bytes 6291460
  14.7 0.7 copy-start.3
  15.4 0.7 copy-start.4
  16.1 0.7 copy-start.5
  16.8 0.6 copy-start.6
  17.4 0.6 copy-start.11

commit v2 on v1

v2 whole, which is shorter than its diff:
```python
import functools

import jax
import jax.numpy as jnp
import numpy as np
from jax import lax
from jax.experimental import pallas as pl
from jax.experimental.pallas import tpu as pltpu
from jax.sharding import PartitionSpec as P

GRID_W = 64
NORM_EPS = 1e-06
ROPE_BASE = 10000.0
HD = 128
CAP = 4
N_DEV = 128
ROWS = 512
TOK = 128
D = 2048
FF = 512
SEQ = 16384
SCALE_LOG2E = float(HD**-0.5 * np.log2(np.e))
KEY_BLOCK = 2048
MESH = pl.DeviceIdType.MESH
VMEM = pl.BlockSpec(memory_space=pltpu.VMEM)
ANY = pl.BlockSpec(memory_space=pl.ANY)
HBM = pl.BlockSpec(memory_space=pltpu.HBM)


def angle_tables():
    quarter = HD // 4
    freq = (ROPE_BASE ** (-np.arange(quarter, dtype=np.float64) / quarter)).astype(np.float32)

    def pair(count, at):
        angles = np.arange(count, dtype=np.float32)[:, None] * freq[None, :]
        cos = np.zeros((count, HD), np.float32)
        sin = np.zeros((count, HD), np.float32)
        c, s = np.cos(angles.astype(np.float64)), np.sin(angles.astype(np.float64))
        cos[:, at : at + quarter] = c
        cos[:, 64 + at : 64 + at + quarter] = c
        sin[:, at : at + quarter] = -s
        sin[:, 64 + at : 64 + at + quarter] = s
        return cos, sin

    return pair(SEQ // GRID_W, 0) + pair(GRID_W, quarter)


def arrivals():
    def of(o1, o2):
        parts = (0, 1) if (o1 == 2 or o2 == 2) else (None,)
        return [(p, o1, o2, part) for p in (0, 1) for part in parts]

    order = []
    for o1, o2 in [
        (-1, 0), (1, 0), (0, -1), (0, 1), (2, 0),
        (-1, -1), (1, 1), (-1, 1), (1, -1), (0, 2),
        (2, -1), (2, 1), (-1, 2), (1, 2), (2, 2),
    ]:
        order += of(o1, o2)
    return order


ARRIVALS = arrivals()
SEM_OF = {a: i for i, a in enumerate(ARRIVALS)}

SCHEDULE = (
    ("rows", 0),
    ("relay", 1),
    ("rows", 1),
    ("relay", 2),
    ("rows", 2),
    ("queries", 0),
    ("relay", 3),
    ("rows", 3),
    ("attend", 0),
    ("relay", 4),
    ("experts", 0),
    ("experts", 1),
    ("experts", 2),
    ("experts", 3),
    ("attend", 1),
    ("attend", -1),
    ("attend", 2),
)


def main_kernel(
    q_hbm, k_hbm, v_hbm, qg_hbm, kg_hbm, rc_hbm, rs_hbm, cc_hbm, cs_hbm,
    tok_hbm, ng_hbm, routes_hbm, gp_hbm, lg_hbm, wg_hbm, wu_hbm, wd_hbm, op_hbm,
    a_hbm, b_hbm,
    q_ref, k_ref, qg_ref, kg_ref, rc_ref, rs_ref, cc_ref, cs_ref,
    tok_ref, ng_ref, routes_ref, gp_ref, lg_ref,
    rows_ref, qr_ref, pick_ref, w_ref, a_buf, b_buf, b_sum,
    kvbuf, arrived, sent, ret, acc, att_out, att_in, wg, wu, wd, op,
    w_sem, in_sem, disp_send, disp_recv, ret_send, ret_recv,
    kv_send, kv_recv, d2d_send, d2d_recv, att_send, att_recv,
):
    f32, bf16 = jnp.float32, jnp.bfloat16
    ep, tp = lax.axis_index("ep"), lax.axis_index("tp")
    z, y, c = ep // 8, (ep // 2) % 4, ep % 2
    g = (tp + y + z) % 4
    me = g * 32 + ep
    partner = ep + 1 - 2 * c
    own_rows = pl.ds(pl.multiple_of(ep * ROWS, ROWS), ROWS)
    grid_rows = ROWS // GRID_W
    here = pl.ds(pl.multiple_of(ep * grid_rows, grid_rows), grid_rows)

    barrier = pltpu.get_barrier_semaphore()

    def greet(k, _):
        to = (ep ^ (k // 4), tp ^ (k % 4))
        pl.semaphore_signal(barrier, 1, device_id=to, device_id_type=MESH)
        return 0

    lax.fori_loop(1, N_DEV, greet, 0)

    takes = [
        (k_hbm, k_ref), (kg_hbm, kg_ref), (rc_hbm.at[here], rc_ref), (rs_hbm.at[here], rs_ref),
        (cc_hbm, cc_ref), (cs_hbm, cs_ref), (v_hbm, kvbuf.at[own_rows, pl.ds(HD, HD)]),
        (q_hbm, q_ref), (qg_hbm, qg_ref),
        (tok_hbm, tok_ref), (ng_hbm, ng_ref), (routes_hbm, routes_ref), (gp_hbm, gp_ref),
        (lg_hbm, lg_ref),
    ]
    takes = [pltpu.make_async_copy(x, to, in_sem.at[i]) for i, (x, to) in enumerate(takes)]
    for take in takes:
        take.start()

    loads = [
        pltpu.make_async_copy(wg_hbm.at[0], wg, w_sem.at[0]),
        pltpu.make_async_copy(wu_hbm.at[0], wu, w_sem.at[1]),
        pltpu.make_async_copy(wd_hbm.at[0], wd, w_sem.at[2]),
        pltpu.make_async_copy(op_hbm, op, w_sem.at[3]),
    ]
    def remote(src, dst, send, recv, to):
        return pltpu.make_async_remote_copy(
            src_ref=src, dst_ref=dst, send_sem=send, recv_sem=recv,
            device_id=to, device_id_type=MESH,
        )

    for take in takes[:7]:
        take.wait()
    cos = (rc_ref[...][:, None, :] + cc_ref[...][None, :, :]).reshape(ROWS, HD)
    sin = (rs_ref[...][:, None, :] + cs_ref[...][None, :, :]).reshape(ROWS, HD)

    def turned(x, gain):
        x = x.astype(f32)
        x = x * lax.rsqrt(jnp.mean(x * x, axis=-1, keepdims=True) + NORM_EPS) * gain
        return (x * cos + pltpu.roll(x, 64, 1) * sin).astype(bf16)

    kvbuf[own_rows, :HD] = turned(k_ref[...], kg_ref[...])
    pl.semaphore_wait(barrier, N_DEV - 1)
    def moved(p, ring, step):
        if (ring == 0) == (p == 0):
            return ((z * 4 + (y + step + 4) % 4) * 2 + c, tp)
        return ((((z + step + 4) % 4) * 4 + y) * 2 + c, tp)

    def owner_rows(p, o1, o2, part):
        dy, dz = (o1, o2) if p == 0 else (o2, o1)
        owner = (((z + dz + 4) % 4) * 4 + (y + dy + 4) % 4) * 2 + c
        start = owner * ROWS + p * 256 + (0 if part is None else part * 128)
        size = 256 if part is None else 128
        return pl.ds(pl.multiple_of(start, 128), size)

    def kv_copy(p, o1, o2, part, arrival, to):
        at = kvbuf.at[owner_rows(p, o1, o2, part)]
        return remote(at, at, kv_send, kv_recv.at[SEM_OF[arrival]], to)

    def to_partner(p, o1, o2, part, sem):
        at = kvbuf.at[owner_rows(p, o1, o2, part)]
        return remote(at, at, d2d_send, d2d_recv.at[sem], (partner, tp))

    def start_own():
        for p in (0, 1):
            for ring in (0, 1):
                for step in (1, -1):
                    arrival = (p, -step, 0, None) if ring == 0 else (p, 0, -step, None)
                    kv_copy(p, 0, 0, None, arrival, moved(p, ring, step)).start()
        for p in (0, 1):
            to_partner(p, 0, 0, None, len(ARRIVALS) + p).start()

    def relay(a):
        p, o1, o2, part = a
        kv_copy(p, o1, o2, part, a, (partner, tp)).wait_recv()
        if o2 == 0 and o1 in (-1, 1):
            half = 0 if o1 == -1 else 1
            kv_copy(p, o1, 0, half, (p, 2, 0, half), moved(p, 0, -o1)).start()
        if o2 == 0:
            for step in (1, -1):
                kv_copy(p, o1, 0, part, (p, o1, -step, part), moved(p, 1, step)).start()
        if o2 in (-1, 1):
            half = 0 if o2 == -1 else 1
            if part is None or part == half:
                kv_copy(p, o1, o2, half, (p, o1, 2, half), moved(p, 1, -o2)).start()
        to_partner(p, o1, o2, part, SEM_OF[a]).start()

    def pick_rows():
        for take in takes[9:]:
            take.wait()
        lane = lax.broadcasted_iota(jnp.int32, (TOK, N_DEV), 1)
        sub = lax.broadcasted_iota(jnp.int32, (TOK, N_DEV), 0)
        diagonal = sub == lane

        def column(row):
            return jnp.sum(jnp.where(diagonal, row, 0.0), axis=1, keepdims=True)

        wide = tok_ref[...].astype(f32)
        normed = (
            wide * lax.rsqrt(jnp.mean(wide * wide, axis=-1, keepdims=True) + NORM_EPS) * ng_ref[...]
        ).astype(bf16)
        routed = routes_ref[...].astype(f32)
        r0 = column(routed[0:1]).astype(jnp.int32)
        r1 = column(routed[1:2]).astype(jnp.int32)
        hot0 = (lane == r0).astype(f32)
        hot1 = (lane == r1).astype(f32)
        before = (sub > lane).astype(f32).astype(bf16)
        count0 = jnp.dot(before, hot0.astype(bf16), preferred_element_type=f32)
        count1 = jnp.dot(before, hot1.astype(bf16), preferred_element_type=f32)
        count1 = count1 + jnp.sum(hot0, axis=0, keepdims=True)
        rank0 = jnp.sum(count0 * hot0, axis=1, keepdims=True)
        rank1 = jnp.sum(count1 * hot1, axis=1, keepdims=True)
        slots = lax.broadcasted_iota(jnp.int32, (TOK, N_DEV * CAP), 1)

        def place(e):
            return (((e & 3) + ((e >> 3) & 3) + (e >> 5)) & 3) * 32 + (e >> 2)

        c0 = (slots == place(r0) * CAP + rank0.astype(jnp.int32)).astype(f32)
        c1 = (slots == place(r1) * CAP + rank1.astype(jnp.int32)).astype(f32)
        pick_ref[:TOK] = c0.astype(bf16)
        pick_ref[TOK:] = c1.astype(bf16)
        picked = lax.dot_general(
            (c0 + c1).astype(bf16), normed, (((0,), (0,)), ((), ())), preferred_element_type=f32
        ).astype(bf16)
        rows_ref[...] = picked.reshape(N_DEV, CAP, D)
        l0, l1 = lg_ref[0:1], lg_ref[1:2]
        top = jnp.maximum(l0, l1)
        e0, e1 = jnp.exp(l0 - top), jnp.exp(l1 - top)
        w_ref[:, 0:1] = column(gp_ref[...] * (e0 / (e0 + e1)))
        w_ref[:, 1:2] = column(gp_ref[...] * (e1 / (e0 + e1)))
        arrived[me] = rows_ref[me]

    def dispatch(jd, first, last):
        def send(m, _):
            k = (m * 11) % 32
            z2, y2, c2 = (z + k // 8) % 4, (y + (k // 2) % 4) % 4, (c + k % 2) % 2
            x2 = (g + jd + 8 - y2 - z2) % 4
            e2 = (z2 * 4 + y2) * 2 + c2
            remote(
                rows_ref.at[((g + jd) % 4) * 32 + e2], arrived.at[me],
                disp_send, disp_recv.at[(4 - jd) % 4], (e2, x2),
            ).start()
            return 0

        lax.fori_loop(first, last, send, 0)

    def experts(j):
        count = 31 if j == 0 else 32
        span = pl.ds(0, count)
        remote(
            rows_ref.at[span], arrived.at[span], disp_send, disp_recv.at[j], (partner, tp)
        ).wait_recv()
        group = (g + j) % 4
        at = pl.ds(pl.multiple_of(group * 32, 32), 32)
        x = arrived[at].reshape(32 * CAP, D)
        gate = jnp.dot(x, wg[...], preferred_element_type=f32)
        up = jnp.dot(x, wu[...], preferred_element_type=f32)
        hidden = (gate / (1.0 + jnp.exp(-gate)) * up).astype(bf16)
        out = jnp.dot(hidden, wd[...], preferred_element_type=f32).astype(bf16)
        sent[at] = out.reshape(32, CAP, D)

    def give_back(j):
        if j == 0:
            ret[me] = sent[me]

        def send(m, _):
            k = (m * 11) % 32
            z2, y2, c2 = (z + k // 8) % 4, (y + (k // 2) % 4) % 4, (c + k % 2) % 2
            x2 = (g + j + 8 - y2 - z2) % 4
            e2 = (z2 * 4 + y2) * 2 + c2
            remote(
                sent.at[((g + j) % 4) * 32 + e2], ret.at[me],
                ret_send, ret_recv.at[(4 - j) % 4], (e2, x2),
            ).start()
            return 0

        lax.fori_loop(1 if j == 0 else 0, 32, send, 0)

    def combine(j):
        count = 31 if j == 0 else 32
        span = pl.ds(0, count)
        remote(
            sent.at[span], ret.at[span], ret_send, ret_recv.at[j], (partner, tp)
        ).wait_recv()
        group = (g + j) % 4
        back = ret[pl.ds(pl.multiple_of(group * 32, 32), 32)].reshape(32 * CAP, D)
        pick = pick_ref[:, pl.ds(pl.multiple_of(group * 128, 128), 128)]
        picked = jnp.dot(pick, back, preferred_element_type=f32)
        part = picked[:TOK] * w_ref[:, 0:1] + picked[TOK:] * w_ref[:, 1:2]
        if j == 0:
            b_sum[...] = part
        else:
            b_sum[...] += part

    ones = jnp.ones((KEY_BLOCK, HD), bf16)

    def attend(dz):
        if dz == 0:
            for p in (0, 1):
                to_partner(p, 0, 0, None, len(ARRIVALS) + p).wait_recv()
        for a in ARRIVALS:
            if (a[2] if a[0] == 0 else a[1]) == dz:
                to_partner(*a, SEM_OF[a]).wait_recv()
        plane = ((z + dz + 4) % 4) * (8 * ROWS)

        def block(i, _):
            at = pl.ds(pl.multiple_of(plane + i * KEY_BLOCK, KEY_BLOCK), KEY_BLOCK)
            key = kvbuf[at, :HD]
            value = jnp.concatenate([kvbuf[at, HD:], ones], axis=1)
            for t in range(4):
                rows = pl.ds(t * 256, 256)
                s = lax.dot_general(
                    qr_ref[rows], key, (((1,), (1,)), ((), ())), preferred_element_type=f32
                )
                weights = jnp.exp2(s * SCALE_LOG2E).astype(bf16)
                acc[rows] += jnp.dot(weights, value, preferred_element_type=f32)
            return 0

        lax.fori_loop(0, 8 * ROWS // KEY_BLOCK, block, 0)

    start_own()
    for load in loads:
        load.start()
    pick_rows()
    for kind, at in SCHEDULE:
        if kind == "queries":
            for take in takes[7:9]:
                take.wait()
            qr_ref[:ROWS] = turned(q_ref[:, :HD], qg_ref[...])
            qr_ref[ROWS:] = turned(q_ref[:, HD:], qg_ref[...])
            acc[...] = jnp.zeros_like(acc)
        elif kind == "rows":
            dispatch((4 - at) % 4, 1 if at == 0 else 0, 32)
        elif kind == "relay":
            for a in ARRIVALS:
                if abs(a[1]) + abs(a[2]) == at:
                    relay(a)
        elif kind == "experts":
            if at == 0:
                for load in loads[:3]:
                    load.wait()
            experts(at)
            give_back(at)
        else:
            attend(at)

    for t in range(4):
        for h in range(2):
            part = acc[pl.ds(h * ROWS + t * TOK, TOK)]
            att_out[t, :, h * HD : (h + 1) * HD] = (part[:, :HD] / part[:, HD:]).astype(bf16)
    for step in (1, 2, 3):
        to = (tp + step) % 4
        remote(att_out.at[to], att_in.at[tp], att_send, att_recv, (ep, to)).start()
    att_in[tp] = att_out[tp]
    for j in (0, 3, 2):
        combine(j)
    loads[3].wait()
    span = pl.ds(0, 3)
    remote(att_out.at[span], att_in.at[span], att_send, att_recv, (partner, tp)).wait_recv()
    total = jnp.dot(att_in[0], op[0:256], preferred_element_type=f32)
    for t in range(1, 4):
        total += jnp.dot(att_in[t], op[t * 256 : (t + 1) * 256], preferred_element_type=f32)
    a_buf[...] = total.astype(bf16)
    out_a = pltpu.make_async_copy(a_buf, a_hbm, w_sem.at[4])
    out_a.start()
    combine(1)
    b_buf[...] = b_sum[...].astype(bf16)
    out_b = pltpu.make_async_copy(b_buf, b_hbm, w_sem.at[5])
    out_b.start()
    span = pl.ds(0, N_DEV - 1)

    remote(
        rows_ref.at[span], arrived.at[span], disp_send, ret_recv.at[0], (partner, tp)
    ).wait_send()
    remote(sent.at[span], ret.at[span], ret_send, ret_recv.at[0], (partner, tp)).wait_send()
    remote(
        kvbuf.at[pl.ds(0, 15 * ROWS)], kvbuf.at[pl.ds(0, 15 * ROWS)],
        kv_send, kv_recv.at[0], (partner, tp),
    ).wait_send()
    remote(
        kvbuf.at[pl.ds(0, 16 * ROWS)], kvbuf.at[pl.ds(0, 16 * ROWS)],
        d2d_send, d2d_recv.at[0], (partner, tp),
    ).wait_send()
    three = pl.ds(0, 3)
    remote(att_out.at[three], att_in.at[three], att_send, att_recv, (partner, tp)).wait_send()
    out_a.wait()
    out_b.wait()


def final_kernel(a_in, b_in, a_out, b_out, held, sem):
    ins = [pltpu.make_async_copy(x, held.at[i], sem.at[i]) for i, x in enumerate((a_in, b_in))]
    outs = [
        pltpu.make_async_copy(held.at[i], x, sem.at[2 + i]) for i, x in enumerate((a_out, b_out))
    ]
    for copy in ins:
        copy.start()
    for i in (0, 1):
        ins[i].wait()
        outs[i].start()
    for copy in outs:
        copy.wait()


def body(
    queries, keys, values, query_gain, key_gain, out_proj, tokens_b, norm_gain, routes,
    group_prob, expert_logits, w_gate, w_up, w_down,
):
    bf16, f32 = jnp.bfloat16, jnp.float32
    tables = [jnp.asarray(t) for t in angle_tables()]
    out, buf = jax.ShapeDtypeStruct, pltpu.VMEM
    dma, many = pltpu.SemaphoreType.DMA, len(ARRIVALS)
    mixed = pl.pallas_call(
        main_kernel,
        out_shape=(out((TOK, D), bf16), out((TOK, D), bf16)),
        in_specs=[ANY] * 18,
        out_specs=(HBM, HBM),
        scratch_shapes=[
            buf((ROWS, 2 * HD), bf16), buf((ROWS, HD), bf16), buf((1, HD), f32), buf((1, HD), f32),
            buf((ROWS // GRID_W, HD), f32), buf((ROWS // GRID_W, HD), f32),
            buf((GRID_W, HD), f32), buf((GRID_W, HD), f32),
            buf((TOK, D), bf16), buf((1, D), f32), buf((2, TOK), jnp.int32), buf((1, TOK), f32),
            buf((2, TOK), f32),
            buf((N_DEV, CAP, D), bf16), buf((2 * ROWS, HD), bf16),
            buf((2 * TOK, N_DEV * CAP), bf16), buf((TOK, 2), f32),
            buf((TOK, D), bf16), buf((TOK, D), bf16), buf((TOK, D), f32),
            buf((SEQ, 2 * HD), bf16),
            buf((N_DEV, CAP, D), bf16), buf((N_DEV, CAP, D), bf16), buf((N_DEV, CAP, D), bf16),
            buf((2 * ROWS, 2 * HD), f32),
            buf((4, TOK, 2 * HD), bf16), buf((4, TOK, 2 * HD), bf16),
            buf((D, FF), bf16), buf((D, FF), bf16), buf((FF, D), bf16), buf((8 * HD, D), bf16),
            dma((6,)), dma((14,)), dma, dma((4,)), dma, dma((4,)),
            dma, dma((many,)), dma, dma((many + 2,)), dma, dma,
        ],
        compiler_params=pltpu.CompilerParams(
            collective_id=0, has_side_effects=True, vmem_limit_bytes=60 << 20
        ),
    )(
        queries, keys, values, query_gain.reshape(1, HD), key_gain.reshape(1, HD), *tables,
        tokens_b, norm_gain.reshape(1, D), routes.T, group_prob.reshape(1, TOK),
        expert_logits.T, w_gate, w_up, w_down, out_proj,
    )
    return pl.pallas_call(
        final_kernel,
        out_shape=(out((TOK, D), bf16), out((TOK, D), bf16)),
        in_specs=[HBM] * 2,
        out_specs=(HBM,) * 2,
        scratch_shapes=[buf((2, TOK, D), bf16), dma((4,))],
        compiler_params=pltpu.CompilerParams(vmem_limit_bytes=60 << 20),
    )(*mixed)


def solution(mesh):
    both = P(("ep", "tp"), None)
    placed = (
        P("ep", "tp"),
        P("ep", "tp"),
        P("ep", "tp"),
        P(),
        P(),
        P(),
        both,
        P(),
        both,
        P(("ep", "tp")),
        both,
        P(("ep", "tp"), None, None),
        P(("ep", "tp"), None, None),
        P(("ep", "tp"), None, None),
    )
    return jax.shard_map(
        body, mesh=mesh, in_specs=placed, out_specs=(both, both), check_vma=False
    )
```

time: 118 us -> 90.6 us (0.77)
  local copies, waits for them, and re-layouts: 19.8 us -> 0 us
  Pallas kernels: 97.4 us -> 89.6 us
    unnamed x40 -> x0, local copies, waits for them, and re-layouts: 19.8 us -> none
    pallas_call x1, Pallas kernels: 96 us -> 87.6 us  [body(): pl.pallas_call(main_kernel, out_shape=(out((TOK, D), bf16), out((TOK, D),...]
where the time goes in v2:
time: 90.6 us; the launch traced here: 90.4 us
  Pallas kernels  89.6 us (99%)
    pallas_call x1, Pallas kernels, body(): pl.pallas_call(main_kernel, out_shape=(out((TOK, D), bf16), out((TOK, D),...  87.6 us
    pallas_call x1, Pallas kernels, body(): pl.pallas_call(final_kernel, out_shape=(out((TOK, D), bf16), out((TOK, D)...  2.04 us

profile of v2, /device:TPU:0, one launch (start us, length us, event | category | flops | bytes accessed | tf_op | source)
XLA Modules:
  0.0 90.4 jit_solution(7996195751080129626)
XLA Ops:
  0.6 87.6 %shard_map.185 = (bf16[128,2048]{1,0:T(8,128)(2,1)}, bf16[128,2048]{1,0:T(8,128)(2,1)}) custom-call(bf16[512,256]{1,0:T(8,128)(2,1)} %q_hbm.1, bf16[512,128]{1,0:T(8,128)(2,1)} %k_hbm.1, bf16[512,128]{1,0:T(8,128)(2,1)} %v_hbm.1, f32[1,128]{1,0:T(1,128)} %bitcast.9, f32[1,128]{1,0:T(1,128)} %bitcast.10, f32[256,128]{1,0:T(8,128)} %constant.8.clone.rc_hbm, ...), custom_call_target="tpu_custom_call" | custom-call | tf_op jit(solution)/shard_map/pallas_call | solution.py:420
  88.2 2.0 %shard_map.186 = (bf16[128,2048]{1,0:T(8,128)(2,1)}, bf16[128,2048]{1,0:T(8,128)(2,1)}) custom-call(bf16[128,2048]{1,0:T(8,128)(2,1)} %get-tuple-element.4.a_in, bf16[128,2048]{1,0:T(8,128)(2,1)} %get-tuple-element.5.b_in), custom_call_target="tpu_custom_call" | custom-call | tf_op jit(solution)/shard_map/pallas_call | solution.py:450

commit v3 on v2

--- a/solution.py
+++ b/solution.py
@@ -76,9 +76,9 @@
     ("relay", 4),
     ("experts", 0),
     ("experts", 1),
+    ("attend", 1),
     ("experts", 2),
     ("experts", 3),
-    ("attend", 1),
     ("attend", -1),
     ("attend", 2),
 )
@@ -93,7 +93,7 @@
     rows_ref, qr_ref, pick_ref, w_ref, a_buf, b_buf, b_sum,
     kvbuf, arrived, sent, ret, acc, att_out, att_in, wg, wu, wd, op,
     w_sem, in_sem, disp_send, disp_recv, ret_send, ret_recv,
-    kv_send, kv_recv, d2d_send, d2d_recv, att_send, att_recv,
+    kv_send, kv_recv, d2d_send, d2d_recv, att_send, att_recv, round_sem,
 ):
     f32, bf16 = jnp.float32, jnp.bfloat16
     ep, tp = lax.axis_index("ep"), lax.axis_index("tp")
@@ -107,12 +107,16 @@
 
     barrier = pltpu.get_barrier_semaphore()
 
-    def greet(k, _):
-        to = (ep ^ (k // 4), tp ^ (k % 4))
-        pl.semaphore_signal(barrier, 1, device_id=to, device_id_type=MESH)
-        return 0
-
-    lax.fori_loop(1, N_DEV, greet, 0)
+    kin = [(ep, (tp + step) % 4) for step in (1, 3, 2)]
+    kin += [((z * 4 + (y + step) % 4) * 2 + c, tp) for step in (1, 3, 2)]
+    kin += [((((z + step) % 4) * 4 + y) * 2 + c, tp) for step in (1, 3, 2)]
+    kin += [(partner, tp)]
+
+    def tell(sem):
+        for to in kin:
+            pl.semaphore_signal(sem, 1, device_id=to, device_id_type=MESH)
+
+    tell(barrier)
 
     takes = [
         (k_hbm, k_ref), (kg_hbm, kg_ref), (rc_hbm.at[here], rc_ref), (rs_hbm.at[here], rs_ref),
@@ -148,7 +152,9 @@
         return (x * cos + pltpu.roll(x, 64, 1) * sin).astype(bf16)
 
     kvbuf[own_rows, :HD] = turned(k_ref[...], kg_ref[...])
-    pl.semaphore_wait(barrier, N_DEV - 1)
+    pl.semaphore_wait(barrier, len(kin))
+    tell(round_sem.at[0])
+
     def moved(p, ring, step):
         if (ring == 0) == (p == 0):
             return ((z * 4 + (y + step + 4) % 4) * 2 + c, tp)
@@ -327,9 +333,13 @@
         lax.fori_loop(0, 8 * ROWS // KEY_BLOCK, block, 0)
 
     start_own()
+    for step in (0, 1):
+        pl.semaphore_wait(round_sem.at[step], len(kin))
+        tell(round_sem.at[step + 1])
     for load in loads:
         load.start()
     pick_rows()
+    pl.semaphore_wait(round_sem.at[2], len(kin))
     for kind, at in SCHEDULE:
         if kind == "queries":
             for take in takes[7:9]:
@@ -438,6 +448,7 @@
             buf((D, FF), bf16), buf((D, FF), bf16), buf((FF, D), bf16), buf((8 * HD, D), bf16),
             dma((6,)), dma((14,)), dma, dma((4,)), dma, dma((4,)),
             dma, dma((many,)), dma, dma((many + 2,)), dma, dma,
+            pltpu.SemaphoreType.REGULAR((3,)),
         ],
         compiler_params=pltpu.CompilerParams(
             collective_id=0, has_side_effects=True, vmem_limit_bytes=60 << 20

time: 90.6 us -> 87.1 us (0.961)
  Pallas kernels: 89.6 us -> 86.2 us
    pallas_call x1, Pallas kernels: 87.6 us -> 84.1 us  [body(): pl.pallas_call(main_kernel, out_shape=(out((TOK, D), bf16), out((TOK, D),...]
where the time goes in v3:
time: 87.1 us; the launch traced here: 87 us
  Pallas kernels  86.2 us (99%)
    pallas_call x1, Pallas kernels, body(): pl.pallas_call(main_kernel, out_shape=(out((TOK, D), bf16), out((TOK, D),...  84.1 us
    pallas_call x1, Pallas kernels, body(): pl.pallas_call(final_kernel, out_shape=(out((TOK, D), bf16), out((TOK, D)...  2.04 us

profile of v3, /device:TPU:0, one launch (start us, length us, event | category | flops | bytes accessed | tf_op | source)
XLA Modules:
  0.0 87.0 jit_solution(9267818675640414849)
XLA Ops:
  0.6 84.1 %shard_map.185 = (bf16[128,2048]{1,0:T(8,128)(2,1)}, bf16[128,2048]{1,0:T(8,128)(2,1)}) custom-call(bf16[512,256]{1,0:T(8,128)(2,1)} %q_hbm.1, bf16[512,128]{1,0:T(8,128)(2,1)} %k_hbm.1, bf16[512,128]{1,0:T(8,128)(2,1)} %v_hbm.1, f32[1,128]{1,0:T(1,128)} %bitcast.9, f32[1,128]{1,0:T(1,128)} %bitcast.10, f32[256,128]{1,0:T(8,128)} %constant.8.clone.rc_hbm, ...), custom_call_target="tpu_custom_call" | custom-call | tf_op jit(solution)/shard_map/pallas_call | solution.py:430
  84.8 2.0 %shard_map.186 = (bf16[128,2048]{1,0:T(8,128)(2,1)}, bf16[128,2048]{1,0:T(8,128)(2,1)}) custom-call(bf16[128,2048]{1,0:T(8,128)(2,1)} %get-tuple-element.4.a_in, bf16[128,2048]{1,0:T(8,128)(2,1)} %get-tuple-element.5.b_in), custom_call_target="tpu_custom_call" | custom-call | tf_op jit(solution)/shard_map/pallas_call | solution.py:461

commit v4 on v3

--- a/solution.py
+++ b/solution.py
@@ -116,6 +116,10 @@
         for to in kin:
             pl.semaphore_signal(sem, 1, device_id=to, device_id_type=MESH)
 
+    def next_round(step):
+        pl.semaphore_wait(round_sem.at[step], len(kin))
+        tell(round_sem.at[step + 1])
+
     tell(barrier)
 
     takes = [
@@ -233,6 +237,7 @@
         c1 = (slots == place(r1) * CAP + rank1.astype(jnp.int32)).astype(f32)
         pick_ref[:TOK] = c0.astype(bf16)
         pick_ref[TOK:] = c1.astype(bf16)
+        next_round(1)
         picked = lax.dot_general(
             (c0 + c1).astype(bf16), normed, (((0,), (0,)), ((), ())), preferred_element_type=f32
         ).astype(bf16)
@@ -333,11 +338,9 @@
         lax.fori_loop(0, 8 * ROWS // KEY_BLOCK, block, 0)
 
     start_own()
-    for step in (0, 1):
-        pl.semaphore_wait(round_sem.at[step], len(kin))
-        tell(round_sem.at[step + 1])
     for load in loads:
         load.start()
+    next_round(0)
     pick_rows()
     pl.semaphore_wait(round_sem.at[2], len(kin))
     for kind, at in SCHEDULE:

time: 87.1 us -> 87.4 us (level)
  no operation moved by 1% of the time
where the time goes in v4:
time: 87.4 us; the launch traced here: 87.2 us
  Pallas kernels  86.4 us (99%)
    pallas_call x1, Pallas kernels, body(): pl.pallas_call(main_kernel, out_shape=(out((TOK, D), bf16), out((TOK, D),...  84.4 us
    pallas_call x1, Pallas kernels, body(): pl.pallas_call(final_kernel, out_shape=(out((TOK, D), bf16), out((TOK, D)...  2.04 us

profile of v4, /device:TPU:0, one launch (start us, length us, event | category | flops | bytes accessed | tf_op | source)
XLA Modules:
  0.0 87.2 jit_solution(8317731561470517552)
XLA Ops:
  0.6 84.4 %shard_map.185 = (bf16[128,2048]{1,0:T(8,128)(2,1)}, bf16[128,2048]{1,0:T(8,128)(2,1)}) custom-call(bf16[512,256]{1,0:T(8,128)(2,1)} %q_hbm.1, bf16[512,128]{1,0:T(8,128)(2,1)} %k_hbm.1, bf16[512,128]{1,0:T(8,128)(2,1)} %v_hbm.1, f32[1,128]{1,0:T(1,128)} %bitcast.9, f32[1,128]{1,0:T(1,128)} %bitcast.10, f32[256,128]{1,0:T(8,128)} %constant.8.clone.rc_hbm, ...), custom_call_target="tpu_custom_call" | custom-call | tf_op jit(solution)/shard_map/pallas_call | solution.py:433
  85.0 2.0 %shard_map.186 = (bf16[128,2048]{1,0:T(8,128)(2,1)}, bf16[128,2048]{1,0:T(8,128)(2,1)}) custom-call(bf16[128,2048]{1,0:T(8,128)(2,1)} %get-tuple-element.4.a_in, bf16[128,2048]{1,0:T(8,128)(2,1)} %get-tuple-element.5.b_in), custom_call_target="tpu_custom_call" | custom-call | tf_op jit(solution)/shard_map/pallas_call | solution.py:464
